TPU v7x, 128 devices: a whole 4x4x4 slice. The times are simulated.
128 devices in a mesh: fs: 32 (over z, y, core), tp: 4 (over x).
Axes of the slice: x: 4, y: 4, z: 4, core: 2. Of those that a mesh axis runs over, the one named last changes fastest.
Arguments:
- model_input: bfloat16 [65536, 2048], P('fs'), may hold values from -6 to 6
- value_cotan: bfloat16 [65536, 2048], P('fs', 'tp'), may hold values from -0.0234375 to 0.0234375
- mixer_cotan: bfloat16 [65536, 2048], P('fs'), may hold values from -0.0234375 to 0.0234375
- head_output: bfloat16 [65536, 2048], P('fs', 'tp'), may hold values from -6 to 6
- value_weight: float32 [2048, 2048], P('fs', 'tp'), may hold values from -0.125 to 0.125
- value_factor: bfloat16 [2048, 512], P('fs'), may hold values from -0.125 to 0.125
- value_first: float32 [512, 2048], P('fs', 'tp'), may hold values from -3 to 3
- value_second: float32 [512, 2048], P('fs', 'tp'), may hold values from 0.02 to 0.5
- output_weight: float32 [2048, 2048], P('fs', 'tp'), may hold values from -0.125 to 0.125
- output_factor: bfloat16 [2048, 512], P('fs'), may hold values from -0.125 to 0.125
- output_first: float32 [512, 2048], P('fs', 'tp'), may hold values from -3 to 3
- output_second: float32 [512, 2048], P('fs', 'tp'), may hold values from 0.02 to 0.5
Outputs:
- value_step: float32 [2048, 2048], P('fs', 'tp')
- value_updated: float32 [2048, 2048], P('fs', 'tp')
- value_first_new: float32 [512, 2048], P('fs', 'tp')
- value_second_new: float32 [512, 2048], P('fs', 'tp')
- value_copy: bfloat16 [2048, 2048], P(None, 'tp')
- output_step: float32 [2048, 2048], P('fs', 'tp')
- output_updated: float32 [2048, 2048], P('fs', 'tp')
- output_first_new: float32 [512, 2048], P('fs', 'tp')
- output_second_new: float32 [512, 2048], P('fs', 'tp')
- output_copy: bfloat16 [2048, 2048], P(None, 'tp')
All inputs are finite; a program needn't handle non-finite values.
Results may differ from a plain program's by a relative error of at most 0.0059.
Values may be sent and summed in bfloat16 or wider, within the bound.
No kernel may reach another device: no remote copies, remote signals or barrier semaphores. Data moves between devices by JAX's collectives and lax.ppermute only.
A program may use at most 128 MiB of HBM per device.

v0:
```python
import jax
import jax.numpy as jnp
from jax import lax
from jax.sharding import Mesh
from jax.sharding import PartitionSpec as P

D = 2048
HV = 2048
FS = ("fs_0", "fs_1", "fs_2")
FS_TP = ("fs_0", "fs_1", "fs_2", "tp")
beta_first = 0.8
beta_second = 0.9
step_rate = 0.02
scale_floor = 0.25
tiny_eps = 1e-08


def sent_to_all(x, axis):
    copies = jnp.broadcast_to(x, (lax.axis_size(axis), *x.shape))
    return lax.all_to_all(copies, axis, split_axis=0, concat_axis=0, tiled=True)


def joined_along(parts, dim):
    dims = list(parts.shape[1:])
    dims[dim] *= parts.shape[0]
    return jnp.moveaxis(parts, 0, dim).reshape(dims)


def gathered_copies(x, axis, dim):
    parts = sent_to_all(x, axis)
    return joined_along(parts, dim)


def cut_along(x, dim, length):
    before, after = (x.shape[:dim], x.shape[dim + 1 :])
    return jnp.moveaxis(x.reshape(*before, length, -1, *after), dim, 0)


def sent_and_summed(x, axis, dim):
    parts = cut_along(x, dim, lax.axis_size(axis))
    arrived = lax.all_to_all(parts, axis, split_axis=0, concat_axis=0, tiled=True)
    return arrived.astype(jnp.float32).sum(axis=0)


def one_axis_at_a_time(x, axes):
    for axis in axes:
        x = lax.psum(x, axis)
    return x


def sent_together(arrays, axis, dim, along):
    ends, at = ([], 0)
    for a in arrays[:-1]:
        at += a.shape[along]
        ends.append(at)
    both = jnp.concatenate(arrays, axis=along)
    return tuple(jnp.split(lax.all_gather(both, axis, axis=dim, tiled=True), ends, axis=along))


def low_rank(rows_in, cols_in, factor, first_moment, second_moment):
    token_dims = (((0,), (0,)), ((), ()))
    reduced = jnp.dot(rows_in, gathered_copies(factor, FS, 0), preferred_element_type=jnp.float32)
    reduced_high = lax.optimization_barrier(reduced.astype(jnp.bfloat16))
    reduced_low = (reduced - reduced_high.astype(jnp.float32)).astype(jnp.bfloat16)
    high_part = lax.dot_general(
        reduced_high, cols_in, token_dims, preferred_element_type=jnp.float32
    )
    low_part = lax.dot_general(reduced_low, cols_in, token_dims, preferred_element_type=jnp.float32)
    projected = sent_and_summed((high_part + low_part).astype(jnp.bfloat16), FS, 0)
    first_new = beta_first * first_moment + (1.0 - beta_first) * projected
    second_new = beta_second * second_moment + (1.0 - beta_second) * projected * projected
    direction = (first_new / (jnp.sqrt(second_new) + tiny_eps)).astype(jnp.bfloat16)
    expanded = jnp.dot(
        factor, gathered_copies(direction, FS, 0), preferred_element_type=jnp.float32
    )
    return (expanded, first_new, second_new)


def local(
    model_input,
    value_cotan,
    mixer_cotan,
    head_output,
    value_weight,
    value_factor,
    value_first,
    value_second,
    output_weight,
    output_factor,
    output_first,
    output_second,
):
    value_exp, value_fnew, value_snew = low_rank(
        model_input, value_cotan, value_factor, value_first, value_second
    )
    output_exp, output_fnew, output_snew = low_rank(
        mixer_cotan, head_output, output_factor, output_first, output_second
    )
    value_sq, output_sq = (
        one_axis_at_a_time(jnp.sum(value_exp * value_exp), FS_TP),
        one_axis_at_a_time(jnp.sum(output_exp * output_exp), FS_TP),
    )
    value_step = step_rate / jnp.sqrt(value_sq / (D * HV) + scale_floor) * value_exp
    output_step = step_rate / jnp.sqrt(output_sq / (D * HV) + scale_floor) * output_exp
    value_updated = value_weight - value_step
    output_updated = output_weight - output_step
    value_copy, output_copy = sent_together(
        (value_updated.astype(jnp.bfloat16), output_updated.astype(jnp.bfloat16)), FS, 0, 1
    )
    return (
        value_step,
        value_updated,
        value_fnew,
        value_snew,
        value_copy,
        output_step,
        output_updated,
        output_fnew,
        output_snew,
        output_copy,
    )


def solution(mesh):
    torus = Mesh(mesh.devices.reshape(4, 4, 2, mesh.shape["tp"]), ("fs_0", "fs_1", "fs_2", "tp"))
    in_specs = (
        P(FS, None),
        P(FS, "tp"),
        P(FS, None),
        P(FS, "tp"),
        P(FS, "tp"),
        P(FS, None),
        P(FS, "tp"),
        P(FS, "tp"),
        P(FS, "tp"),
        P(FS, None),
        P(FS, "tp"),
        P(FS, "tp"),
    )
    out_specs = (
        P(FS, "tp"),
        P(FS, "tp"),
        P(FS, "tp"),
        P(FS, "tp"),
        P(None, "tp"),
        P(FS, "tp"),
        P(FS, "tp"),
        P(FS, "tp"),
        P(FS, "tp"),
        P(None, "tp"),
    )
    return jax.shard_map(local, mesh=torus, in_specs=in_specs, out_specs=out_specs, check_vma=False)
```

profile of v0, /device:TPU:1, one launch (start us, length us, event | category | flops | bytes accessed | tf_op | source)
XLA Modules:
  0.0 239.8 jit_solution(17554075201442228649)
XLA Ops:
  7.2 0.0 copy-start
  7.2 1.2 broadcast_in_dim.12
  8.4 0.0 copy-start.3
  8.4 37.9 %all_to_all.30 = bf16[32,64,512]{2,1,0:T(8,128)(2,1)} all-to-all(bf16[32,64,512]{2,1,0:T(8,128)(2,1)S(1)} %broadcast_in_dim.12), channel_id=1, replica_groups=mesh['fs_0'=4,'fs_1'=4,'fs_2'=2,'tp'=4] {'fs_0','fs_1','fs_2'}, dimensions={0} | all-to-all | bytes 4194304 | tf_op jit(solution)/shard_map/all_to_all | solution.py:20
  46.3 0.0 copy-done.3
  46.3 1.6 broadcast_in_dim.14
  47.9 4.8 %all-to-all-start.3 = ((bf16[32,64,512]{2,1,0:T(8,128)(2,1)}), bf16[32,64,512]{2,1,0:T(8,128)(2,1)}, u32[]{:S(2)}, u32[]{:S(2)}) async-start(bf16[32,64,512]{2,1,0:T(8,128)(2,1)} %broadcast_in_dim.14), calls=%async_computation.3 | async-start | bytes 4194304 | tf_op jit(solution)/shard_map/all_to_all | solution.py:20
  52.7 7.6 %fusion.13 = (bf16[2048,512]{1,0:T(8,128)(2,1)S(1)}, f32[2048,512]{1,0:T(8,128)S(1)}) fusion(bf16[2048,2048]{1,0:T(8,128)(2,1)} %param.12, bf16[2048,512]{1,0:T(8,128)(2,1)} %bitcast.26), kind=kOutput, calls=%fused_computation.26 | convolution fusion | flops 4296015872 | bytes 16777216 | tf_op jit(solution)/shard_map/dot_general | solution.py:62
  60.2 0.0 copy-done
  60.2 1.3 fusion.15
  61.5 2.2 fusion.4
  63.7 17.3 %all-to-all-done.3 = bf16[32,64,512]{2,1,0:T(8,128)(2,1)} async-done(((bf16[32,64,512]{2,1,0:T(8,128)(2,1)}), bf16[32,64,512]{2,1,0:T(8,128)(2,1)}, u32[]{:S(2)}, u32[]{:S(2)}) %all-to-all-start.3) | async-done | bytes 2097184 | tf_op jit(solution)/shard_map/all_to_all | solution.py:20
  81.0 5.7 %all-to-all-start.1 = ((bf16[32,16,512]{2,1,0:T(8,128)(2,1)}), bf16[32,16,512]{2,1,0:T(8,128)(2,1)S(1)}, u32[]{:S(2)}, u32[]{:S(2)}) async-start(bf16[32,16,512]{2,1,0:T(8,128)(2,1)} %bitcast.1), calls=%async_computation.1 | async-start | bytes 1048576 | tf_op jit(solution)/shard_map/all_to_all | solution.py:41
  86.7 0.0 copy-start.1
  86.7 7.7 %fusion.14 = (bf16[2048,512]{1,0:T(8,128)(2,1)S(1)}, f32[2048,512]{1,0:T(8,128)S(1)}) fusion(bf16[2048,2048]{1,0:T(8,128)(2,1)} %param.14, bf16[2048,512]{1,0:T(8,128)(2,1)} %bitcast.4), kind=kOutput, calls=%fused_computation.27 | convolution fusion | flops 4296015872 | bytes 16777216 | tf_op jit(solution)/shard_map/dot_general | solution.py:62
  94.4 1.3 fusion.16
  95.7 0.0 copy-start.5
  95.7 0.0 copy-start.6
  95.7 2.1 fusion.5
  97.8 0.4 all-to-all-done.1
  98.2 7.1 %all-to-all-start.4 = ((bf16[32,16,512]{2,1,0:T(8,128)(2,1)}), bf16[32,16,512]{2,1,0:T(8,128)(2,1)S(1)}, u32[]{:S(2)}, u32[]{:S(2)}) async-start(bf16[32,16,512]{2,1,0:T(8,128)(2,1)} %bitcast.5), calls=%async_computation.4 | async-start | bytes 1048576 | tf_op jit(solution)/shard_map/all_to_all | solution.py:41
  105.3 0.1 convert_reduce_fusion.1
  105.4 0.0 copy-done.5
  105.4 0.0 copy-done.6
  105.4 0.0 copy-start.2
  105.4 0.6 divide_convert_fusion.1
  106.1 10.7 %all-to-all-done.4 = bf16[32,16,512]{2,1,0:T(8,128)(2,1)S(1)} async-done(((bf16[32,16,512]{2,1,0:T(8,128)(2,1)}), bf16[32,16,512]{2,1,0:T(8,128)(2,1)S(1)}, u32[]{:S(2)}, u32[]{:S(2)}) %all-to-all-start.4) | async-done | bytes 524320 | tf_op jit(solution)/shard_map/all_to_all | solution.py:41
  116.7 0.9 broadcast_in_dim.13
  117.6 3.9 %all-to-all-start.2 = ((bf16[32,16,512]{2,1,0:T(8,128)(2,1)}), bf16[32,16,512]{2,1,0:T(8,128)(2,1)S(1)}, u32[]{:S(2)}, u32[]{:S(2)}) async-start(bf16[32,16,512]{2,1,0:T(8,128)(2,1)} %broadcast_in_dim.13), calls=%async_computation.2 | async-start | bytes 1048576 | tf_op jit(solution)/shard_map/all_to_all | solution.py:20
  121.5 0.0 copy-start.4
  121.5 0.1 convert_reduce_fusion
  121.6 1.4 divide_convert_fusion
  123.0 10.0 %all-to-all-done.2 = bf16[32,16,512]{2,1,0:T(8,128)(2,1)S(1)} async-done(((bf16[32,16,512]{2,1,0:T(8,128)(2,1)}), bf16[32,16,512]{2,1,0:T(8,128)(2,1)S(1)}, u32[]{:S(2)}, u32[]{:S(2)}) %all-to-all-start.2) | async-done | bytes 524320 | tf_op jit(solution)/shard_map/all_to_all | solution.py:20
  133.1 0.9 broadcast_in_dim.15
  133.9 3.9 %all-to-all-start.5 = ((bf16[32,16,512]{2,1,0:T(8,128)(2,1)}), bf16[32,16,512]{2,1,0:T(8,128)(2,1)S(1)}, u32[]{:S(2)}, u32[]{:S(2)}) async-start(bf16[32,16,512]{2,1,0:T(8,128)(2,1)} %broadcast_in_dim.15), calls=%async_computation.5 | async-start | bytes 1048576 | tf_op jit(solution)/shard_map/all_to_all | solution.py:20
  137.9 0.0 all-gather.2.cloned.1.call-start
  137.9 0.8 multiply_reduce_fusion.1
  138.8 10.7 %all-to-all-done.5 = bf16[32,16,512]{2,1,0:T(8,128)(2,1)S(1)} async-done(((bf16[32,16,512]{2,1,0:T(8,128)(2,1)}), bf16[32,16,512]{2,1,0:T(8,128)(2,1)S(1)}, u32[]{:S(2)}, u32[]{:S(2)}) %all-to-all-start.5) | async-done | bytes 524320 | tf_op jit(solution)/shard_map/all_to_all | solution.py:20
  149.4 0.8 multiply_reduce_fusion
  150.2 7.4 %all-reduce.2 = (f32[]{:T(128)}, f32[]{:T(128)}) all-reduce(f32[]{:T(128)} %get-tuple-element.34, f32[]{:T(128)} %get-tuple-element.38), channel_id=1, replica_groups=mesh['fs_0'=4,'fs_1'=4,'fs_2'=2,'tp'=4] {'fs_0'}, use_global_device_ids=true, to_apply=%region_2.0 | all-reduce | flops 2 | bytes 16 | tf_op jit(solution)/shard_map/psum | solution.py:47
  157.7 8.5 %all-reduce.1 = (f32[]{:T(128)}, f32[]{:T(128)}) all-reduce(f32[]{:T(128)} %get-tuple-element.14, f32[]{:T(128)} %get-tuple-element.15), channel_id=1, replica_groups=mesh['fs_0'=4,'fs_1'=4,'fs_2'=2,'tp'=4] {'fs_1'}, use_global_device_ids=true, to_apply=%region_3.0 | all-reduce | flops 2 | bytes 16 | tf_op jit(solution)/shard_map/psum | solution.py:47
  166.1 5.8 %all-reduce.3 = (f32[]{:T(128)}, f32[]{:T(128)}) all-reduce(f32[]{:T(128)} %get-tuple-element.12, f32[]{:T(128)} %get-tuple-element.13), channel_id=1, replica_groups=mesh['fs_0'=4,'fs_1'=4,'fs_2'=2,'tp'=4] {'fs_2'}, use_global_device_ids=true, to_apply=%region_4.0 | all-reduce | flops 2 | bytes 16 | tf_op jit(solution)/shard_map/psum | solution.py:47
  171.9 9.1 %all-reduce = (f32[]{:T(128)}, f32[]{:T(128)}) all-reduce(f32[]{:T(128)} %get-tuple-element.16, f32[]{:T(128)} %get-tuple-element.17), channel_id=1, replica_groups=mesh['fs_0'=4,'fs_1'=4,'fs_2'=2,'tp'=4] {'tp'}, use_global_device_ids=true, to_apply=%region_5.0 | all-reduce | flops 2 | bytes 16 | tf_op jit(solution)/shard_map/psum | solution.py:47
  182.4 1.7 fusion.8
  184.1 0.7 pad_maximum_fusion
  184.8 0.0 all-gather.2.cloned.1.call-update
  184.8 43.6 %all-gather.2.cloned.1.call-done = bf16[2048,1024]{1,0:T(8,128)(2,1)} async-done(((bf16[64,1024]{1,0:T(8,128)(2,1)}), bf16[2048,1024]{1,0:T(8,128)(2,1)}) %all-gather.2.cloned.1.call-update) | async-done | bytes 4194320 | tf_op jit(solution)/shard_map/all_gather | solution.py:57
  228.4 4.5 %fusion.12 = (bf16[2048,512]{1,0:T(8,128)(2,1)}, bf16[2048,512]{1,0:T(8,128)(2,1)}) fusion(bf16[2048,1024]{1,0:T(8,128)(2,1)} %all-gather.2.cloned.1.call-done), kind=kLoop, calls=%fused_computation.25 | loop fusion | bytes 8388608 | tf_op jit(solution)/shard_map/split | solution.py:57
  (3 shorter events, 0.0 us)
Async XLA Ops:
  7.2 53.1 %copy-start = (bf16[2048,512]{1,0:T(8,128)(2,1)S(1)}, bf16[2048,512]{1,0:T(8,128)(2,1)}, u32[]{:S(2)}) copy-start(bf16[2048,512]{1,0:T(8,128)(2,1)} %param.13) | copy-start | bytes 6291460
  8.4 37.9 %copy-start.3 = (bf16[64,512]{1,0:T(8,128)(2,1)S(1)}, bf16[64,512]{1,0:T(8,128)(2,1)}, u32[]{:S(2)}) copy-start(bf16[64,512]{1,0:T(8,128)(2,1)} %param.21) | copy-start | bytes 196612
  47.9 33.1 %all-to-all-start.3 = ((bf16[32,64,512]{2,1,0:T(8,128)(2,1)}), bf16[32,64,512]{2,1,0:T(8,128)(2,1)}, u32[]{:S(2)}, u32[]{:S(2)}) async-start(bf16[32,64,512]{2,1,0:T(8,128)(2,1)} %broadcast_in_dim.14), calls=%async_computation.3 | async-start | bytes 4194304 | tf_op jit(solution)/shard_map/all_to_all | solution.py:20
  81.0 17.2 %all-to-all-start.1 = ((bf16[32,16,512]{2,1,0:T(8,128)(2,1)}), bf16[32,16,512]{2,1,0:T(8,128)(2,1)S(1)}, u32[]{:S(2)}, u32[]{:S(2)}) async-start(bf16[32,16,512]{2,1,0:T(8,128)(2,1)} %bitcast.1), calls=%async_computation.1 | async-start | bytes 1048576 | tf_op jit(solution)/shard_map/all_to_all | solution.py:41
  86.7 7.7 %copy-start.1 = (bf16[2048,512]{1,0:T(8,128)(2,1)S(1)}, bf16[2048,512]{1,0:T(8,128)(2,1)}, u32[]{:S(2)}) copy-start(bf16[2048,512]{1,0:T(8,128)(2,1)} %param.15) | copy-start | bytes 6291460
  95.7 9.7 %copy-start.5 = (f32[16,512]{1,0:T(8,128)S(1)}, f32[16,512]{1,0:T(8,128)}, u32[]{:S(2)}) copy-start(f32[16,512]{1,0:T(8,128)} %param.19) | copy-start | bytes 98308
  95.7 9.7 %copy-start.6 = (f32[16,512]{1,0:T(8,128)S(1)}, f32[16,512]{1,0:T(8,128)}, u32[]{:S(2)}) copy-start(f32[16,512]{1,0:T(8,128)} %param.18) | copy-start | bytes 98308
  98.2 18.5 %all-to-all-start.4 = ((bf16[32,16,512]{2,1,0:T(8,128)(2,1)}), bf16[32,16,512]{2,1,0:T(8,128)(2,1)S(1)}, u32[]{:S(2)}, u32[]{:S(2)}) async-start(bf16[32,16,512]{2,1,0:T(8,128)(2,1)} %bitcast.5), calls=%async_computation.4 | async-start | bytes 1048576 | tf_op jit(solution)/shard_map/all_to_all | solution.py:41
  105.4 32.5 %copy-start.2 = (bf16[64,512]{1,0:T(8,128)(2,1)S(1)}, bf16[64,512]{1,0:T(8,128)(2,1)}, u32[]{:S(2)}) copy-start(bf16[64,512]{1,0:T(8,128)(2,1)} %param.17) | copy-start | bytes 196612
  117.6 15.5 %all-to-all-start.2 = ((bf16[32,16,512]{2,1,0:T(8,128)(2,1)}), bf16[32,16,512]{2,1,0:T(8,128)(2,1)S(1)}, u32[]{:S(2)}, u32[]{:S(2)}) async-start(bf16[32,16,512]{2,1,0:T(8,128)(2,1)} %broadcast_in_dim.13), calls=%async_computation.2 | async-start | bytes 1048576 | tf_op jit(solution)/shard_map/all_to_all | solution.py:20
  121.5 60.9 %copy-start.4 = (f32[64,512]{1,0:T(8,128)S(1)}, f32[64,512]{1,0:T(8,128)}, u32[]{:S(2)}) copy-start(f32[64,512]{1,0:T(8,128)} %param.16) | copy-start | bytes 393220
  133.9 15.5 %all-to-all-start.5 = ((bf16[32,16,512]{2,1,0:T(8,128)(2,1)}), bf16[32,16,512]{2,1,0:T(8,128)(2,1)S(1)}, u32[]{:S(2)}, u32[]{:S(2)}) async-start(bf16[32,16,512]{2,1,0:T(8,128)(2,1)} %broadcast_in_dim.15), calls=%async_computation.5 | async-start | bytes 1048576 | tf_op jit(solution)/shard_map/all_to_all | solution.py:20
  137.9 90.5 %all-gather.2.cloned.1.call-start = ((), (), s32[]{:S(2)}) async-start(), calls=%async_computation.6 | async-start | bytes 4325376 | tf_op jit(solution)/shard_map/all_gather | solution.py:57
Sparse Core Ops, SparseCore 0:
  184.9 43.4 all-gather.1
where the time goes:
time: 241 us; the launch traced here: 240 us
  waiting for transfers between devices  92.7 us (38%)
  blocking collectives  68.7 us (29%)
  starting transfers between devices  25.4 us (11%)
  matrix products  23.7 us (10%)
  between operations  15.6 us (6%)
  local copies, waits for them, and re-layouts  9.02 us (4%)
  other arithmetic  4.61 us (2%)
    all_gather x1, waiting for transfers between devices, sent_together(): lax.all_gather(both, axis, axis=dim, tiled=True)  43.6 us
    all_to_all x3, waiting for transfers between devices, sent_to_all(): return lax.all_to_all(copies, axis, split_axis=0, concat_axis=0, tiled=True)  38 us
    all_to_all x1, blocking collectives, sent_to_all(): return lax.all_to_all(copies, axis, split_axis=0, concat_axis=0, tiled=True)  37.9 us
    psum x4, blocking collectives, one_axis_at_a_time(): x = lax.psum(x, axis)  30.8 us
    dot_general x2, matrix products, low_rank(): jnp.dot(rows_in, gathered_copies(factor, FS, 0), preferred_element_type=j...  15.2 us
    all_to_all x2, starting transfers between devices, sent_and_summed(): lax.all_to_all(parts, axis, split_axis=0, concat_axis=0, tiled=True)  12.7 us
    all_to_all x3, starting transfers between devices, sent_to_all(): return lax.all_to_all(copies, axis, split_axis=0, concat_axis=0, tiled=True)  12.6 us
    all_to_all x2, waiting for transfers between devices, sent_and_summed(): lax.all_to_all(parts, axis, split_axis=0, concat_axis=0, tiled=True)  11.1 us
  transfers between devices with their start and end apart: 6, of which 6 were waited for; matrix products, arithmetic and copies ran while one was open for 10% of the time, Pallas kernels for 0%

commit v1 on v0

--- a/solution.py
+++ b/solution.py
@@ -44,7 +44,7 @@
 
 def one_axis_at_a_time(x, axes):
     for axis in axes:
-        x = lax.psum(x, axis)
+        x = jnp.sum(lax.all_gather(x, axis), axis=0)
     return x
 
 

time: 241 us -> 256 us (1.062)
  local copies, waits for them, and re-layouts: 9.02 us -> 22.6 us
  other arithmetic: 4.61 us -> 9.42 us
  blocking collectives: 68.7 us -> 66.1 us
    psum x4 -> x0, blocking collectives: 30.8 us -> none  [one_axis_at_a_time(): x = lax.psum(x, axis)]
    unnamed x0 -> x4, blocking collectives: none -> 28.2 us
    unnamed x14 -> x42, local copies, waits for them, and re-layouts: 0.05 us -> 13.6 us
    reduce_sum x0 -> x8, other arithmetic: none -> 4.81 us  [one_axis_at_a_time(): x = jnp.sum(lax.all_gather(x, axis), axis=0)]
where the time goes in v1:
time: 256 us; the launch traced here: 255 us
  waiting for transfers between devices  92.1 us (36%)
  blocking collectives  66.1 us (26%)
  starting transfers between devices  25.4 us (10%)
  matrix products  23.7 us (9%)
  local copies, waits for them, and re-layouts  22.6 us (9%)
  between operations  15.7 us (6%)
  other arithmetic  9.42 us (4%)
    all_gather x1, waiting for transfers between devices, sent_together(): lax.all_gather(both, axis, axis=dim, tiled=True)  43.6 us
    all_to_all x1, blocking collectives, sent_to_all(): return lax.all_to_all(copies, axis, split_axis=0, concat_axis=0, tiled=True)  37.9 us
    all_to_all x3, waiting for transfers between devices, sent_to_all(): return lax.all_to_all(copies, axis, split_axis=0, concat_axis=0, tiled=True)  37.4 us
    unnamed x4, blocking collectives  28.2 us
    dot_general x2, matrix products, low_rank(): jnp.dot(rows_in, gathered_copies(factor, FS, 0), preferred_element_type=j...  15.2 us
    unnamed x42, local copies, waits for them, and re-layouts  13.6 us
    all_to_all x2, starting transfers between devices, sent_and_summed(): lax.all_to_all(parts, axis, split_axis=0, concat_axis=0, tiled=True)  12.7 us
    all_to_all x3, starting transfers between devices, sent_to_all(): return lax.all_to_all(copies, axis, split_axis=0, concat_axis=0, tiled=True)  12.6 us
  transfers between devices with their start and end apart: 6, of which 6 were waited for; matrix products, arithmetic and copies ran while one was open for 10% of the time, Pallas kernels for 0%

profile of v1, /device:TPU:1, one launch (start us, length us, event | category | flops | bytes accessed | tf_op | source)
XLA Modules:
  0.0 255.0 jit_solution(18097167298260419503)
XLA Ops:
  7.2 1.2 broadcast_in_dim.12
  8.4 37.9 %all_to_all.30 = bf16[32,64,512]{2,1,0:T(8,128)(2,1)} all-to-all(bf16[32,64,512]{2,1,0:T(8,128)(2,1)S(1)} %broadcast_in_dim.12), channel_id=1, replica_groups=mesh['fs_0'=4,'fs_1'=4,'fs_2'=2,'tp'=4] {'fs_0','fs_1','fs_2'}, dimensions={0} | all-to-all | bytes 4194304 | tf_op jit(solution)/shard_map/all_to_all | solution.py:20
  46.3 1.6 broadcast_in_dim.14
  47.9 4.7 %all-to-all-start.3 = ((bf16[32,64,512]{2,1,0:T(8,128)(2,1)}), bf16[32,64,512]{2,1,0:T(8,128)(2,1)}, u32[]{:S(2)}, u32[]{:S(2)}) async-start(bf16[32,64,512]{2,1,0:T(8,128)(2,1)} %broadcast_in_dim.14), calls=%async_computation.3 | async-start | bytes 4194304 | tf_op jit(solution)/shard_map/all_to_all | solution.py:20
  52.6 7.6 %fusion.13 = (bf16[2048,512]{1,0:T(8,128)(2,1)S(1)}, f32[2048,512]{1,0:T(8,128)S(1)}) fusion(bf16[2048,2048]{1,0:T(8,128)(2,1)} %param.12, bf16[2048,512]{1,0:T(8,128)(2,1)} %bitcast.38), kind=kOutput, calls=%fused_computation.26 | convolution fusion | flops 4296015872 | bytes 16777216 | tf_op jit(solution)/shard_map/dot_general | solution.py:62
  60.2 1.3 fusion.15
  61.5 2.2 fusion.4
  63.7 17.3 %all-to-all-done.3 = bf16[32,64,512]{2,1,0:T(8,128)(2,1)} async-done(((bf16[32,64,512]{2,1,0:T(8,128)(2,1)}), bf16[32,64,512]{2,1,0:T(8,128)(2,1)}, u32[]{:S(2)}, u32[]{:S(2)}) %all-to-all-start.3) | async-done | bytes 2097184 | tf_op jit(solution)/shard_map/all_to_all | solution.py:20
  81.0 5.7 %all-to-all-start.1 = ((bf16[32,16,512]{2,1,0:T(8,128)(2,1)}), bf16[32,16,512]{2,1,0:T(8,128)(2,1)S(1)}, u32[]{:S(2)}, u32[]{:S(2)}) async-start(bf16[32,16,512]{2,1,0:T(8,128)(2,1)} %bitcast.1), calls=%async_computation.1 | async-start | bytes 1048576 | tf_op jit(solution)/shard_map/all_to_all | solution.py:41
  86.7 7.7 %fusion.14 = (bf16[2048,512]{1,0:T(8,128)(2,1)S(1)}, f32[2048,512]{1,0:T(8,128)S(1)}) fusion(bf16[2048,2048]{1,0:T(8,128)(2,1)} %param.14, bf16[2048,512]{1,0:T(8,128)(2,1)} %bitcast.12), kind=kOutput, calls=%fused_computation.27 | convolution fusion | flops 4296015872 | bytes 16777216 | tf_op jit(solution)/shard_map/dot_general | solution.py:62
  94.4 1.3 fusion.16
  95.7 2.1 fusion.5
  98.2 7.1 %all-to-all-start.4 = ((bf16[32,16,512]{2,1,0:T(8,128)(2,1)}), bf16[32,16,512]{2,1,0:T(8,128)(2,1)S(1)}, u32[]{:S(2)}, u32[]{:S(2)}) async-start(bf16[32,16,512]{2,1,0:T(8,128)(2,1)} %bitcast.13), calls=%async_computation.4 | async-start | bytes 1048576 | tf_op jit(solution)/shard_map/all_to_all | solution.py:41
  105.4 0.6 divide_convert_fusion.1
  106.1 10.7 %all-to-all-done.4 = bf16[32,16,512]{2,1,0:T(8,128)(2,1)S(1)} async-done(((bf16[32,16,512]{2,1,0:T(8,128)(2,1)}), bf16[32,16,512]{2,1,0:T(8,128)(2,1)S(1)}, u32[]{:S(2)}, u32[]{:S(2)}) %all-to-all-start.4) | async-done | bytes 524320 | tf_op jit(solution)/shard_map/all_to_all | solution.py:41
  116.7 0.9 broadcast_in_dim.13
  117.6 3.9 %all-to-all-start.2 = ((bf16[32,16,512]{2,1,0:T(8,128)(2,1)}), bf16[32,16,512]{2,1,0:T(8,128)(2,1)S(1)}, u32[]{:S(2)}, u32[]{:S(2)}) async-start(bf16[32,16,512]{2,1,0:T(8,128)(2,1)} %broadcast_in_dim.13), calls=%async_computation.2 | async-start | bytes 1048576 | tf_op jit(solution)/shard_map/all_to_all | solution.py:20
  121.7 1.4 divide_convert_fusion
  123.1 10.0 %all-to-all-done.2 = bf16[32,16,512]{2,1,0:T(8,128)(2,1)S(1)} async-done(((bf16[32,16,512]{2,1,0:T(8,128)(2,1)}), bf16[32,16,512]{2,1,0:T(8,128)(2,1)S(1)}, u32[]{:S(2)}, u32[]{:S(2)}) %all-to-all-start.2) | async-done | bytes 524320 | tf_op jit(solution)/shard_map/all_to_all | solution.py:20
  133.1 0.9 broadcast_in_dim.15
  133.9 3.9 %all-to-all-start.5 = ((bf16[32,16,512]{2,1,0:T(8,128)(2,1)}), bf16[32,16,512]{2,1,0:T(8,128)(2,1)S(1)}, u32[]{:S(2)}, u32[]{:S(2)}) async-start(bf16[32,16,512]{2,1,0:T(8,128)(2,1)} %broadcast_in_dim.15), calls=%async_computation.5 | async-start | bytes 1048576 | tf_op jit(solution)/shard_map/all_to_all | solution.py:20
  138.5 0.8 multiply_reduce_fusion.1
  139.4 10.1 %all-to-all-done.5 = bf16[32,16,512]{2,1,0:T(8,128)(2,1)S(1)} async-done(((bf16[32,16,512]{2,1,0:T(8,128)(2,1)}), bf16[32,16,512]{2,1,0:T(8,128)(2,1)S(1)}, u32[]{:S(2)}, u32[]{:S(2)}) %all-to-all-start.5) | async-done | bytes 524320 | tf_op jit(solution)/shard_map/all_to_all | solution.py:20
  149.4 0.8 multiply_reduce_fusion
  150.2 1.4 dynamic-update-slice
  151.7 1.4 dynamic-update-slice.4
  153.6 6.8 %all-reduce.10 = (f32[4]{0:T(128)S(1)}, f32[4]{0:T(128)S(1)}) all-reduce(f32[4]{0:T(128)S(1)} %dynamic-update-slice, f32[4]{0:T(128)S(1)} %dynamic-update-slice.4), channel_id=1, replica_groups=mesh['fs_0'=4,'fs_1'=4,'fs_2'=2,'tp'=4] {'fs_0'}, use_global_device_ids=true, to_apply=%add | all-reduce | flops 8 | bytes 64
  160.4 0.6 reduce_sum.110
  161.0 0.6 reduce_sum.116
  161.6 1.4 dynamic-update-slice.1
  163.0 1.4 dynamic-update-slice.5
  165.0 7.8 %all-reduce.9 = (f32[4]{0:T(128)S(1)}, f32[4]{0:T(128)S(1)}) all-reduce(f32[4]{0:T(128)S(1)} %dynamic-update-slice.1, f32[4]{0:T(128)S(1)} %dynamic-update-slice.5), channel_id=1, replica_groups=mesh['fs_0'=4,'fs_1'=4,'fs_2'=2,'tp'=4] {'fs_1'}, use_global_device_ids=true, to_apply=%add.1 | all-reduce | flops 8 | bytes 64
  172.9 0.6 reduce_sum.111
  173.5 0.6 reduce_sum.117
  174.1 1.4 dynamic-update-slice.2
  175.5 1.4 dynamic-update-slice.6
  177.5 5.1 %all-reduce.11 = (f32[2]{0:T(128)S(1)}, f32[2]{0:T(128)S(1)}) all-reduce(f32[2]{0:T(128)S(1)} %dynamic-update-slice.2, f32[2]{0:T(128)S(1)} %dynamic-update-slice.6), channel_id=1, replica_groups=mesh['fs_0'=4,'fs_1'=4,'fs_2'=2,'tp'=4] {'fs_2'}, use_global_device_ids=true, to_apply=%add.2 | all-reduce | flops 4 | bytes 32
  182.6 0.6 reduce_sum.112
  183.2 0.6 reduce_sum.118
  183.8 1.4 dynamic-update-slice.3
  185.2 1.4 dynamic-update-slice.7
  186.6 8.4 %all-reduce.8 = (f32[4]{0:T(128)S(1)}, f32[4]{0:T(128)S(1)}) all-reduce(f32[4]{0:T(128)S(1)} %dynamic-update-slice.3, f32[4]{0:T(128)S(1)} %dynamic-update-slice.7), channel_id=1, replica_groups=mesh['fs_0'=4,'fs_1'=4,'fs_2'=2,'tp'=4] {'tp'}, use_global_device_ids=true, to_apply=%add.3 | all-reduce | flops 8 | bytes 64
  195.1 0.6 reduce_sum.113
  196.4 0.6 reduce_sum.119
  197.7 1.7 fusion.8
  199.4 0.7 pad_maximum_fusion
  200.1 43.6 %all-gather.2.cloned.1.call-done = bf16[2048,1024]{1,0:T(8,128)(2,1)} async-done(((bf16[64,1024]{1,0:T(8,128)(2,1)}), bf16[2048,1024]{1,0:T(8,128)(2,1)}) %all-gather.2.cloned.1.call-update) | async-done | bytes 4194320 | tf_op jit(solution)/shard_map/all_gather | solution.py:57
  243.7 4.5 %fusion.12 = (bf16[2048,512]{1,0:T(8,128)(2,1)}, bf16[2048,512]{1,0:T(8,128)(2,1)}) fusion(bf16[2048,1024]{1,0:T(8,128)(2,1)} %all-gather.2.cloned.1.call-done), kind=kLoop, calls=%fused_computation.25 | loop fusion | bytes 8388608 | tf_op jit(solution)/shard_map/split | solution.py:57
  (39 shorter events, 3.1 us)
Async XLA Ops:
  7.2 53.0 %copy-start = (bf16[2048,512]{1,0:T(8,128)(2,1)S(1)}, bf16[2048,512]{1,0:T(8,128)(2,1)}, u32[]{:S(2)}) copy-start(bf16[2048,512]{1,0:T(8,128)(2,1)} %param.13) | copy-start | bytes 6291460
  8.4 37.9 %copy-start.3 = (bf16[64,512]{1,0:T(8,128)(2,1)S(1)}, bf16[64,512]{1,0:T(8,128)(2,1)}, u32[]{:S(2)}) copy-start(bf16[64,512]{1,0:T(8,128)(2,1)} %param.21) | copy-start | bytes 196612
  47.9 33.1 %all-to-all-start.3 = ((bf16[32,64,512]{2,1,0:T(8,128)(2,1)}), bf16[32,64,512]{2,1,0:T(8,128)(2,1)}, u32[]{:S(2)}, u32[]{:S(2)}) async-start(bf16[32,64,512]{2,1,0:T(8,128)(2,1)} %broadcast_in_dim.14), calls=%async_computation.3 | async-start | bytes 4194304 | tf_op jit(solution)/shard_map/all_to_all | solution.py:20
  81.0 17.2 %all-to-all-start.1 = ((bf16[32,16,512]{2,1,0:T(8,128)(2,1)}), bf16[32,16,512]{2,1,0:T(8,128)(2,1)S(1)}, u32[]{:S(2)}, u32[]{:S(2)}) async-start(bf16[32,16,512]{2,1,0:T(8,128)(2,1)} %bitcast.1), calls=%async_computation.1 | async-start | bytes 1048576 | tf_op jit(solution)/shard_map/all_to_all | solution.py:41
  86.7 7.7 %copy-start.1 = (bf16[2048,512]{1,0:T(8,128)(2,1)S(1)}, bf16[2048,512]{1,0:T(8,128)(2,1)}, u32[]{:S(2)}) copy-start(bf16[2048,512]{1,0:T(8,128)(2,1)} %param.15) | copy-start | bytes 6291460
  95.7 9.7 %copy-start.5 = (f32[16,512]{1,0:T(8,128)S(1)}, f32[16,512]{1,0:T(8,128)}, u32[]{:S(2)}) copy-start(f32[16,512]{1,0:T(8,128)} %param.19) | copy-start | bytes 98308
  95.7 9.7 %copy-start.6 = (f32[16,512]{1,0:T(8,128)S(1)}, f32[16,512]{1,0:T(8,128)}, u32[]{:S(2)}) copy-start(f32[16,512]{1,0:T(8,128)} %param.18) | copy-start | bytes 98308
  98.2 18.5 %all-to-all-start.4 = ((bf16[32,16,512]{2,1,0:T(8,128)(2,1)}), bf16[32,16,512]{2,1,0:T(8,128)(2,1)S(1)}, u32[]{:S(2)}, u32[]{:S(2)}) async-start(bf16[32,16,512]{2,1,0:T(8,128)(2,1)} %bitcast.13), calls=%async_computation.4 | async-start | bytes 1048576 | tf_op jit(solution)/shard_map/all_to_all | solution.py:41
  105.4 32.5 %copy-start.10 = (u32[128]{0:T(128)S(1)}, u32[128]{0:T(128)}, u32[]{:S(2)}) copy-start(u32[128]{0:T(128)} %constant.26) | copy-start | bytes 1540
  105.4 33.1 %copy-start.2 = (bf16[64,512]{1,0:T(8,128)(2,1)S(1)}, bf16[64,512]{1,0:T(8,128)(2,1)}, u32[]{:S(2)}) copy-start(bf16[64,512]{1,0:T(8,128)(2,1)} %param.17) | copy-start | bytes 196612
  117.6 15.5 %all-to-all-start.2 = ((bf16[32,16,512]{2,1,0:T(8,128)(2,1)}), bf16[32,16,512]{2,1,0:T(8,128)(2,1)S(1)}, u32[]{:S(2)}, u32[]{:S(2)}) async-start(bf16[32,16,512]{2,1,0:T(8,128)(2,1)} %broadcast_in_dim.13), calls=%async_computation.2 | async-start | bytes 1048576 | tf_op jit(solution)/shard_map/all_to_all | solution.py:20
  121.5 31.5 %copy-start.9 = (u32[128]{0:T(128)S(1)}, u32[128]{0:T(128)}, u32[]{:S(2)}) copy-start(u32[128]{0:T(128)} %constant.31) | copy-start | bytes 1540
  121.5 42.9 %copy-start.8 = (u32[128]{0:T(128)S(1)}, u32[128]{0:T(128)}, u32[]{:S(2)}) copy-start(u32[128]{0:T(128)} %constant.36) | copy-start | bytes 1540
  121.6 55.3 %copy-start.7 = (u32[128]{0:T(128)S(1)}, u32[128]{0:T(128)}, u32[]{:S(2)}) copy-start(u32[128]{0:T(128)} %constant.41) | copy-start | bytes 1540
  121.6 76.1 %copy-start.4 = (f32[64,512]{1,0:T(8,128)S(1)}, f32[64,512]{1,0:T(8,128)}, u32[]{:S(2)}) copy-start(f32[64,512]{1,0:T(8,128)} %param.16) | copy-start | bytes 393220
  133.9 15.5 %all-to-all-start.5 = ((bf16[32,16,512]{2,1,0:T(8,128)(2,1)}), bf16[32,16,512]{2,1,0:T(8,128)(2,1)S(1)}, u32[]{:S(2)}, u32[]{:S(2)}) async-start(bf16[32,16,512]{2,1,0:T(8,128)(2,1)} %broadcast_in_dim.15), calls=%async_computation.5 | async-start | bytes 1048576 | tf_op jit(solution)/shard_map/all_to_all | solution.py:20
  137.9 105.8 %all-gather.2.cloned.1.call-start = ((), (), s32[]{:S(2)}) async-start(), calls=%async_computation.6 | async-start | bytes 4325376 | tf_op jit(solution)/shard_map/all_gather | solution.py:57
Sparse Core Ops, SparseCore 0:
  200.2 43.4 all-gather.1
